TPU v7x, 32 devices: a whole 2x2x4 slice. The times are simulated.
32 devices in a mesh: fs: 8 (over z, x), tp: 4 (over y, core).
Axes of the slice: x: 2, y: 2, z: 4, core: 2. Of those that a mesh axis runs over, the one named last changes fastest.
Arguments:
- tokens: bfloat16 [8192, 2048], P('fs', 'tp'), may hold values from -17 to 17
- first_gain: float32 [2048], replicated, may hold values from 0.1 to 1.9
- first_gate: bfloat16 [2048, 5120], P('fs', 'tp'), may hold values from -0.125 to 0.125
- first_up: bfloat16 [2048, 5120], P('fs', 'tp'), may hold values from -0.125 to 0.125
- first_down: bfloat16 [2048, 5120], P('fs', 'tp'), may hold values from -0.078125 to 0.078125
- mix_gain: float32 [2048], replicated, may hold values from 0.1 to 1.9
- mix_input: bfloat16 [2048, 1024], P('fs', 'tp'), may hold values from -0.125 to 0.125
- mix_branch: bfloat16 [2048, 1024], P('fs', 'tp'), may hold values from -0.125 to 0.125
- conv_weight: bfloat16 [4, 1024], P(None, 'tp'), may hold values from -3 to 3
- rate_weight: bfloat16 [16, 64, 64], P('tp'), may hold values from -0.75 to 0.75
- input_weight: bfloat16 [16, 64, 64], P('tp'), may hold values from -0.75 to 0.75
- decay_param: float32 [1024], P('tp'), may hold values from 3 to 11
- decay_shift: float32 [8192, 16], P('fs', 'tp'), may hold values from -1.5 to 0
- mix_output: bfloat16 [2048, 1024], P('fs', 'tp'), may hold values from -0.1875 to 0.1875
- second_gain: float32 [2048], replicated, may hold values from 0.1 to 1.9
- second_gate: bfloat16 [2048, 5120], P('fs', 'tp'), may hold values from -0.125 to 0.125
- second_up: bfloat16 [2048, 5120], P('fs', 'tp'), may hold values from -0.125 to 0.125
- second_down: bfloat16 [2048, 5120], P('fs', 'tp'), may hold values from -0.078125 to 0.078125
- final_gain: float32 [2048], P('tp'), may hold values from 0.1 to 1.9
Outputs:
- output: bfloat16 [8192, 2048], P('fs', 'tp')
All inputs are finite; a program needn't handle non-finite values.
Results may differ from a plain program's by a relative error of at most 0.019.
Values may be sent and summed in bfloat16 or wider, within the bound.
A program may use at most 128 MiB of HBM per device.

v0:
```python
import functools

import jax
import jax.numpy as jnp
from jax import lax
from jax.experimental import pallas as pl
from jax.experimental.pallas import tpu as pltpu
from jax.sharding import PartitionSpec as P

HEAD_DIM = 64
CONV = 4
norm_eps = 1e-06
rate_scale = 8.0
MESH = pl.DeviceIdType.MESH
F32, BF16 = jnp.float32, jnp.bfloat16
G1, U1, D1, MI, MB, MO, G2, U2, D2A, D2B = range(10)


def tile_of(size, *choices):
    for choice in choices:
        if size % choice == 0:
            return choice
    return size


def negative_expm1(y):
    series = 1.0 + y * (1.0 / 6.0)
    for k in (5, 4, 3, 2):
        series = 1.0 + y * (1.0 / k) * series
    return jnp.where(y > -0.25, -y * series, 1.0 - jnp.exp(y))


def dot(left, right):
    return jnp.dot(left, right, preferred_element_type=F32)


def dot_last(left, right):
    return lax.dot_general(left, right, (((1,), (1,)), ((), ())), preferred_element_type=F32)


def kernel(
    n,
    m,
    tokens,
    first_gate,
    first_up,
    first_down,
    mix_input,
    mix_branch,
    mix_output,
    second_gate,
    second_up,
    second_down,
    first_gain,
    mix_gain,
    second_gain,
    conv_weight,
    rate_weight,
    input_weight,
    decay_param,
    decay_shift,
    stream,
    scale_out,
    w_gate1,
    w_up1,
    w_down1,
    w_in,
    w_branch,
    w_out,
    w_gate2,
    w_up2,
    w_down2,
    gathered,
    normed,
    hidden,
    terms,
    near,
    far,
    mixed,
    lane,
    branch,
    decay,
    drive,
    rate_map,
    input_map,
    square_own,
    square_in,
    ring_send,
    ring_recv,
    own_sem,
    ag_near_send,
    ag_near_recv,
    ag_far_send,
    ag_far_recv,
    rs_near_send,
    rs_near_recv,
    rs_far_send,
    rs_far_recv,
    sq_send,
    sq_recv,
):
    h = n // 2
    chips = m // 2
    q = n // m
    rows, width = stream.shape
    d = width * m
    block = d // n
    units = first_gate.shape[1]
    lanes = mix_input.shape[1]
    fs = lax.axis_index("fs")
    tp = lax.axis_index("tp")
    chip = tp // 2
    core = tp % 2
    partner = tp + 1 - 2 * core
    at = jnp.where(fs % 2 == 0, fs // 2, n - 1 - fs // 2)

    def owner(place):
        p = lax.rem(place + 2 * n, n)
        return jnp.where(p < h, 2 * p, 2 * (n - 1 - p) + 1)

    right, left = owner(at + 1), owner(at - 1)
    half = block // 2
    plan = [
        (first_gate, w_gate1, 0, block),
        (first_up, w_up1, 0, block),
        (first_down, w_down1, 0, block),
        (mix_input, w_in, 0, block),
        (mix_branch, w_branch, 0, block),
        (mix_output, w_out, 0, block),
        (second_gate, w_gate2, 0, block),
        (second_up, w_up2, 0, block),
        (second_down, w_down2, 0, half),
        (second_down, w_down2, half, half),
    ]

    def ring_copy(k, way, step, arriving=False):
        source, buffer, low, count = plan[k]
        sign = -1 if way == 0 else 1
        b = owner(at + sign * (step + 1 if arriving else step))
        if step == h - 1:
            count = count // 2
            low = low + way * count
        place = pl.ds(pl.multiple_of(b * block + low, 16), count)
        if step == 0 and not arriving:
            src = source if count == block else source.at[pl.ds(low, count)]
        else:
            src = buffer.at[place]
        return pltpu.make_async_remote_copy(
            src_ref=src,
            dst_ref=buffer.at[place],
            send_sem=ring_send.at[k, way, step],
            recv_sem=ring_recv.at[k, way, step],
            device_id={"fs": right if way == 0 else left},
            device_id_type=MESH,
        )

    def launch(*ks):
        for k in ks:
            for way in (0, 1):
                ring_copy(k, way, 0).start()

    def serve(k, step):
        for way in (0, 1):
            ring_copy(k, way, step - 1, arriving=True).wait_recv()
            if step < h:
                ring_copy(k, way, step).start()

    barrier = pltpu.get_barrier_semaphore()
    for target in (left, right):
        pl.semaphore_signal(barrier, inc=1, device_id={"fs": target}, device_id_type=MESH)
    for hop in range(1, m):
        pl.semaphore_signal(
            barrier, inc=1, device_id={"tp": lax.rem(tp + hop, m)}, device_id_type=MESH
        )
    pl.semaphore_wait(barrier, 2 + m - 1)

    def columns(index, size):
        return pl.ds(pl.multiple_of(index * size, 128), size)

    def gather_far(phase, hop, source):
        return pltpu.make_async_remote_copy(
            src_ref=source,
            dst_ref=gathered.at[:, columns(tp, width)],
            send_sem=ag_far_send.at[phase, hop],
            recv_sem=ag_far_recv.at[phase, hop],
            device_id={"tp": lax.rem(tp + 2 * hop, m)},
            device_id_type=MESH,
        )

    def gather_near(phase, hop, source=None, arriving=False):
        origin = lax.rem((partner if arriving else tp) - 2 * hop + 2 * m, m)
        place = gathered.at[:, columns(origin, width)]
        return pltpu.make_async_remote_copy(
            src_ref=place if source is None else source,
            dst_ref=place,
            send_sem=ag_near_send.at[phase, hop],
            recv_sem=ag_near_recv.at[phase, hop],
            device_id={"tp": partner},
            device_id_type=MESH,
        )

    def gather_arrived_far(phase, hop):
        origin = lax.rem(tp - 2 * hop + 2 * m, m)
        place = gathered.at[:, columns(origin, width)]
        return pltpu.make_async_remote_copy(
            src_ref=place,
            dst_ref=place,
            send_sem=ag_far_send.at[phase, hop],
            recv_sem=ag_far_recv.at[phase, hop],
            device_id={"tp": origin},
            device_id_type=MESH,
        )

    def gather_start(phase, source):
        for hop in range(1, chips):
            gather_far(phase, hop, source).start()
        gather_near(phase, 0, source).start()

    def gather_forward(phase):
        for hop in range(1, chips):
            gather_arrived_far(phase, hop).wait_recv()
            gather_near(phase, hop).start()

    def gather_finish(phase, source):
        for hop in range(chips):
            gather_near(phase, hop, arriving=True).wait_recv()
            gather_near(phase, hop, source if hop == 0 else None).wait_send()
        for hop in range(1, chips):
            gather_far(phase, hop, source).wait_send()

    def normalise(gain):
        size = tile_of(rows, 64)

        @pl.loop(0, rows // size)
        def _(i):
            place = pl.ds(pl.multiple_of(i * size, size), size)
            values = gathered[place, :].astype(F32)
            scale = lax.rsqrt(jnp.mean(values * values, axis=-1, keepdims=True) + norm_eps)
            normed[place, :] = (values * scale * gain[...]).astype(BF16)

    row_tile = tile_of(rows, 256)
    unit_tile = tile_of(units, 256, 128)

    def hidden_part(gate, up, part, parts):
        count = rows // row_tile * (units // unit_tile) // parts
        across = units // unit_tile

        @pl.loop(part * count, (part + 1) * count)
        def _(i):
            place = pl.ds(pl.multiple_of((i // across) * row_tile, row_tile), row_tile)
            cols = columns(i % across, unit_tile)
            gate_value = dot(normed[place, :], gate[:, cols])
            up_value = dot(normed[place, :], up[:, cols])
            hidden[place, cols] = (jax.nn.silu(gate_value) * up_value).astype(BF16)

    def near_copy(phase, b):
        slot = b // q // 2 * q + b % q
        return pltpu.make_async_remote_copy(
            src_ref=terms.at[:, columns(b, block)],
            dst_ref=near.at[:, columns(slot, block)],
            send_sem=rs_near_send.at[phase, b],
            recv_sem=rs_near_recv.at[phase, slot],
            device_id={"tp": partner},
            device_id_type=MESH,
        )

    def far_copy(phase, b):
        to_chip = b // q // 2
        hop = lax.rem(to_chip - chip + chips, chips)
        slot = (hop - 1) * q + b % q
        return pltpu.make_async_remote_copy(
            src_ref=terms.at[:, columns(b, block)],
            dst_ref=far.at[:, columns(slot, block)],
            send_sem=rs_far_send.at[phase, b],
            recv_sem=rs_far_recv.at[phase, slot],
            device_id={"tp": to_chip * 2 + core},
            device_id_type=MESH,
        )

    def terms_of(phase, left_ref, weight, b):
        weights = pl.ds(pl.multiple_of(b * block, block), block)

        @pl.loop(0, rows // row_tile)
        def _(i):
            place = pl.ds(pl.multiple_of(i * row_tile, row_tile), row_tile)
            value = dot_last(left_ref[place, :], weight[weights, :])
            terms[place, columns(b, block)] = value.astype(BF16)

        @pl.when(b // q % 2 != core)
        def _():
            near_copy(phase, b).start()

    def pass_on(phase, b):
        mine = b // q % 2 == core
        slot = b // q // 2 * q + b % q

        @pl.when(mine)
        def _():
            near_copy(phase, b).wait_recv()

        @pl.when(mine & (b // q // 2 != chip))
        def _():
            @pl.loop(0, rows // row_tile)
            def _(i):
                place = pl.ds(pl.multiple_of(i * row_tile, row_tile), row_tile)
                total = terms[place, columns(b, block)].astype(F32)
                total = total + near[place, columns(slot, block)].astype(F32)
                terms[place, columns(b, block)] = total.astype(BF16)

            far_copy(phase, b).start()

    def blocks_at(step):
        if step == 0:
            return [fs]
        if step == h:
            return [owner(at + h)]
        return [owner(at - step), owner(at + step)]

    def far_arrived(phase, hop, k):
        slot = (hop - 1) * q + k
        place = far.at[:, slot * block : (slot + 1) * block]
        return pltpu.make_async_remote_copy(
            src_ref=place,
            dst_ref=place,
            send_sem=rs_far_send.at[phase, 0],
            recv_sem=rs_far_recv.at[phase, slot],
            device_id={"tp": partner},
            device_id_type=MESH,
        )

    def finish_sum(phase, factor, whole):
        for hop in range(1, chips):
            for k in range(q):
                far_arrived(phase, hop, k).wait_recv()

        @pl.loop(0, rows // row_tile)
        def _(i):
            place = pl.ds(pl.multiple_of(i * row_tile, row_tile), row_tile)
            total = terms[place, columns(tp, width)].astype(F32)
            total = total + near[place, columns(chip, width)].astype(F32)
            for hop in range(1, chips):
                total = total + far[place, (hop - 1) * width : hop * width].astype(F32)
            value = (stream[place, :].astype(F32) + factor * total).astype(BF16)
            stream[place, :] = value
            if whole:
                gathered[place, columns(tp, width)] = value

    def sent_sum(phase):
        for b in range(n):

            @pl.when(b // q % 2 != core)
            def _():
                near_copy(phase, b).wait_send()

            @pl.when((b // q % 2 == core) & (b // q // 2 != chip))
            def _():
                far_copy(phase, b).wait_send()

    gather_start(0, tokens)
    launch(G1, U1)
    own = [
        pltpu.make_async_copy(tokens, stream, own_sem.at[0]),
        pltpu.make_async_copy(tokens, gathered.at[:, columns(tp, width)], own_sem.at[1]),
    ]
    mine = pl.ds(pl.multiple_of(fs * block, block), block)
    for k in range(9):
        source, buffer, _, _ = plan[k]
        own.append(pltpu.make_async_copy(source, buffer.at[mine], own_sem.at[2 + k]))
    for copy in own:
        copy.start()
    rate_map[...] = jnp.zeros_like(rate_map)
    input_map[...] = jnp.zeros_like(input_map)
    for k in range(lanes // HEAD_DIM):
        part = slice(k * HEAD_DIM, (k + 1) * HEAD_DIM)
        rate_map[part, part] = rate_weight[k]
        input_map[part, part] = input_weight[k]
    lane[0:8, :] = jnp.zeros((8, lanes), F32)
    for copy in own:
        copy.wait()

    serve(G1, 1)
    gather_forward(0)
    serve(U1, 1)
    gather_finish(0, tokens)
    normalise(first_gain)
    for step in range(2, h + 1):
        serve(G1, step)
        serve(U1, step)
        if step == h - 1:
            launch(D1)
    launch(MI, MB, MO)
    hidden_part(w_gate1, w_up1, 0, 1)
    for b in blocks_at(0):
        terms_of(0, hidden, w_down1, b)
    for step in range(1, h + 1):
        serve(D1, step)
        for b in blocks_at(step):
            terms_of(0, hidden, w_down1, b)
        for k in (MI, MB, MO):
            serve(k, step)
        for b in blocks_at(step - 1):
            pass_on(0, b)
        if step == h - 1:
            launch(G2, U2)
    for b in blocks_at(h):
        pass_on(0, b)
    finish_sum(0, 0.5, True)
    gather_start(1, stream)
    sent_sum(0)

    queue = [(k, step) for step in range(1, h + 1) for k in (G2, U2)]

    def take(count):
        for _ in range(min(count, len(queue))):
            k, step = queue.pop(0)
            serve(k, step)
            if k == U2 and step == h - 1:
                launch(D2A, D2B)

    take(1)
    gather_forward(1)
    take(1)
    gather_finish(1, stream)
    normalise(mix_gain)

    @pl.loop(0, rows // row_tile)
    def _(i):
        place = pl.ds(pl.multiple_of(i * row_tile, row_tile), row_tile)
        lower = pl.ds(pl.multiple_of(i * row_tile + 8, 8), row_tile)
        value = dot(normed[place, :], w_in[...])
        lane[lower, :] = value.astype(BF16).astype(F32)
        branch[place, :] = dot(normed[place, :], w_branch[...])

    slope = -rate_scale * jnp.log1p(jnp.exp(-decay_param[...]))
    small = tile_of(rows, 128)
    lane_id = lax.broadcasted_iota(jnp.int32, (small, lanes), 1) // HEAD_DIM

    @pl.loop(0, rows // small)
    def _(i):
        place = pl.ds(pl.multiple_of(i * small, small), small)
        upper = lane[pl.ds(pl.multiple_of(i * small, 8), small + 8), :]
        conv_sum = jnp.zeros((small, lanes), F32)
        for k in range(CONV):
            shifted = pltpu.roll(upper, CONV - 1 - k, 0) if k < CONV - 1 else upper
            conv_sum = conv_sum + shifted[8:, :] * conv_weight[k : k + 1, :].astype(F32)
        conv_out = conv_sum.astype(BF16)
        rate = jax.nn.sigmoid(dot(conv_out, rate_map[...]))
        admit = jax.nn.sigmoid(dot(conv_out, input_map[...]))
        shifts = decay_shift[place, :]
        shift = jnp.zeros((small, lanes), F32)
        for k in range(lanes // HEAD_DIM):
            shift = jnp.where(lane_id == k, shifts[:, k : k + 1], shift)
        log_decay = rate * slope + shift
        decay[place, :] = jnp.exp(log_decay)
        drive[place, :] = (
            jnp.sqrt(negative_expm1(2.0 * log_decay)) * admit * conv_out.astype(F32)
        )

    take(1)
    lane_tile = tile_of(lanes, 128)
    row_id = lax.broadcasted_iota(jnp.int32, (rows, lane_tile), 0)

    @pl.loop(0, lanes // lane_tile)
    def _(i):
        cols = columns(i, lane_tile)
        factor, state = decay[:, cols], drive[:, cols]
        reach = 1
        while reach < rows:
            inside = row_id >= reach
            state = factor * jnp.where(inside, pltpu.roll(state, reach, 0), 0.0) + state
            if reach * 2 < rows:
                factor = factor * jnp.where(inside, pltpu.roll(factor, reach, 0), 1.0)
            reach *= 2
        mixed[:, cols] = (state * jax.nn.gelu(branch[:, cols])).astype(BF16)

    take(1)
    for step in range(h + 1):
        for b in blocks_at(step):
            terms_of(1, mixed, w_out, b)
        if step:
            for b in blocks_at(step - 1):
                pass_on(1, b)
    for b in blocks_at(h):
        pass_on(1, b)
    take(1)
    finish_sum(1, 1.0, True)
    gather_start(2, stream)
    sent_sum(1)
    take(1)
    gather_forward(2)
    take(2 * h)
    gather_finish(2, stream)

    normalise(second_gain)
    halves = [(k, step) for step in range(1, h + 1) for k in (D2A, D2B)]
    parts = tile_of(rows // row_tile, 4, 2)
    for part in range(parts):
        serve(*halves.pop(0))
        hidden_part(w_gate2, w_up2, part, parts)
    for b in blocks_at(0):
        terms_of(2, hidden, w_down2, b)
    for step in range(1, h + 1):
        while halves and halves[0][1] <= step:
            serve(*halves.pop(0))
        for b in blocks_at(step):
            terms_of(2, hidden, w_down2, b)
        for b in blocks_at(step - 1):
            pass_on(2, b)
    for b in blocks_at(h):
        pass_on(2, b)
    finish_sum(2, 0.5, False)

    @pl.loop(0, rows // row_tile)
    def _(i):
        place = pl.ds(pl.multiple_of(i * row_tile, row_tile), row_tile)
        values = stream[place, :].astype(F32)
        squares = jnp.sum(values * values, axis=-1, keepdims=True)
        square_own[:, columns(i, row_tile)] = jnp.broadcast_to(squares, (row_tile, 128)).T[:8, :]

    def square_copy(hop):
        return pltpu.make_async_remote_copy(
            src_ref=square_own,
            dst_ref=square_in.at[hop - 1],
            send_sem=sq_send.at[hop],
            recv_sem=sq_recv.at[hop],
            device_id={"tp": lax.rem(tp + hop, m)},
            device_id_type=MESH,
        )

    for hop in range(1, m):
        square_copy(hop).start()
    sent_sum(2)
    for k in range(len(plan)):
        for way in (0, 1):
            for step in range(h):
                ring_copy(k, way, step).wait_send()
    for hop in range(1, m):
        square_copy(hop).wait()

    @pl.loop(0, rows // row_tile)
    def _(i):
        place = pl.ds(pl.multiple_of(i * row_tile, row_tile), row_tile)
        cols = columns(i, row_tile)
        squares = square_own[:, cols]
        for hop in range(1, m):
            squares = squares + square_in[hop - 1, :, cols]
        spread = jnp.broadcast_to(squares[0:1, :], (128, row_tile)).T
        scale_out[place, :] = lax.rsqrt(spread / d + norm_eps)


def shards(n, m, *arrays):
    (
        tokens,
        first_gain,
        first_gate,
        first_up,
        first_down,
        mix_gain,
        mix_input,
        mix_branch,
        conv_weight,
        rate_weight,
        input_weight,
        decay_param,
        decay_shift,
        mix_output,
        second_gain,
        second_gate,
        second_up,
        second_down,
        final_gain,
    ) = arrays
    rows, width = tokens.shape
    d = width * m
    units = first_gate.shape[1]
    lanes = mix_input.shape[1]
    h, q, chips = n // 2, n // m, m // 2
    hbm = pl.BlockSpec(memory_space=pl.ANY)
    vmem = pl.BlockSpec(memory_space=pltpu.VMEM)
    dma = pltpu.SemaphoreType.DMA
    stream, scale = pl.pallas_call(
        functools.partial(kernel, n, m),
        out_shape=(
            jax.ShapeDtypeStruct((rows, width), BF16),
            jax.ShapeDtypeStruct((rows, 128), F32),
        ),
        in_specs=[hbm] * 10 + [vmem] * 8,
        out_specs=(vmem, vmem),
        scratch_shapes=[
            *[pltpu.VMEM((d, units), BF16)] * 3,
            *[pltpu.VMEM((d, lanes), BF16)] * 3,
            *[pltpu.VMEM((d, units), BF16)] * 3,
            pltpu.VMEM((rows, d), BF16),
            pltpu.VMEM((rows, d), BF16),
            pltpu.VMEM((rows, units), BF16),
            pltpu.VMEM((rows, d), BF16),
            pltpu.VMEM((rows, chips * width), BF16),
            pltpu.VMEM((rows, max(chips - 1, 1) * width), BF16),
            pltpu.VMEM((rows, lanes), BF16),
            pltpu.VMEM((rows + 8, lanes), F32),
            pltpu.VMEM((rows, lanes), F32),
            pltpu.VMEM((rows, lanes), F32),
            pltpu.VMEM((rows, lanes), F32),
            pltpu.VMEM((lanes, lanes), BF16),
            pltpu.VMEM((lanes, lanes), BF16),
            pltpu.VMEM((8, rows), F32),
            pltpu.VMEM((m - 1, 8, rows), F32),
            dma((10, 2, h)),
            dma((10, 2, h)),
            dma((11,)),
            dma((3, chips)),
            dma((3, chips)),
            dma((3, chips)),
            dma((3, chips)),
            dma((3, n)),
            dma((3, n // 2)),
            dma((3, n)),
            dma((3, max(chips - 1, 1) * q)),
            dma((m,)),
            dma((m,)),
        ],
        compiler_params=pltpu.CompilerParams(
            collective_id=0, has_side_effects=True, vmem_limit_bytes=67043328
        ),
        cost_estimate=pl.CostEstimate(
            flops=rows * d * (12 * units + 6 * lanes), bytes_accessed=8 * d * units, transcendentals=0
        ),
    )(
        tokens,
        first_gate,
        first_up,
        first_down,
        mix_input,
        mix_branch,
        mix_output,
        second_gate,
        second_up,
        second_down,
        first_gain[None, :],
        mix_gain[None, :],
        second_gain[None, :],
        conv_weight,
        rate_weight,
        input_weight,
        decay_param[None, :],
        decay_shift,
    )
    return (stream.astype(F32) * scale[:, :1] * final_gain).astype(BF16)


def solution(mesh):
    return jax.shard_map(
        functools.partial(shards, mesh.shape["fs"], mesh.shape["tp"]),
        mesh=mesh,
        in_specs=(
            P("fs", "tp"),
            P(),
            P("fs", "tp"),
            P("fs", "tp"),
            P("fs", "tp"),
            P(),
            P("fs", "tp"),
            P("fs", "tp"),
            P(None, "tp"),
            P("tp", None, None),
            P("tp", None, None),
            P("tp"),
            P("fs", "tp"),
            P("fs", "tp"),
            P(),
            P("fs", "tp"),
            P("fs", "tp"),
            P("fs", "tp"),
            P("tp"),
        ),
        out_specs=P("fs", "tp"),
        check_vma=False,
    )
```

profile of v0, /device:TPU:0, one launch (start us, length us, event | category | flops | bytes accessed | tf_op | source)
XLA Modules:
  0.0 375.2 jit_solution(2587000337181112315)
XLA Ops:
  0.0 1.7 copy.21.decay_shift
  1.7 369.7 %shard_map.181 = (bf16[1024,512]{1,0:T(8,128)(2,1)}, f32[1024,128]{1,0:T(8,128)}) custom-call(bf16[1024,512]{1,0:T(8,128)(2,1)} %tokens.1, bf16[256,1280]{1,0:T(8,128)(2,1)} %first_gate.1, bf16[256,1280]{1,0:T(8,128)(2,1)} %first_up.1, bf16[256,1280]{1,0:T(8,128)(2,1)} %first_down.1, bf16[256,256]{1,0:T(8,128)(2,1)} %mix_input.1, ...), custom_call_target="tpu_custom_call" | custom-call | flops 35433480192 | bytes 20971520 | tf_op jit(solution)/shard_map/pallas_call | solution.py:581
  371.5 1.2 slice_reduce_fusion
  372.7 2.5 multiply_convert_fusion
where the time goes:
time: 376 us; the launch traced here: 375 us
  Pallas kernels  370 us (98%)
    pallas_call x1, Pallas kernels, shards(): pl.pallas_call(functools.partial(kernel, n, m), out_shape=(jax.ShapeDtype...  370 us

commit v1 on v0

--- a/solution.py
+++ b/solution.py
@@ -30,6 +30,15 @@
     return jnp.where(y > -0.25, -y * series, 1.0 - jnp.exp(y))
 
 
+def scoped(f):
+    def g(*args):
+        tag = "_".join(str(a) for a in args if isinstance(a, int))
+        with jax.named_scope(f"{f.__name__}_{tag}"):
+            return f(*args)
+
+    return g
+
+
 def dot(left, right):
     return jnp.dot(left, right, preferred_element_type=F32)
 
@@ -41,6 +50,7 @@
 def kernel(
     n,
     m,
+    split,
     tokens,
     first_gate,
     first_up,
@@ -59,8 +69,8 @@
     input_weight,
     decay_param,
     decay_shift,
+    final_gain,
     stream,
-    scale_out,
     w_gate1,
     w_up1,
     w_down1,
@@ -71,11 +81,16 @@
     w_up2,
     w_down2,
     gathered,
+    gathered_mate,
     normed,
+    normed_mate,
     hidden,
-    terms,
+    hidden_half,
     near,
+    near_mate,
     far,
+    far_mate,
+    from_mate,
     mixed,
     lane,
     branch,
@@ -98,6 +113,12 @@
     rs_far_recv,
     sq_send,
     sq_recv,
+    spread_send,
+    spread_recv,
+    cross_send,
+    cross_recv,
+    mate_send,
+    mate_recv,
 ):
     h = n // 2
     chips = m // 2
@@ -119,6 +140,22 @@
         return jnp.where(p < h, 2 * p, 2 * (n - 1 - p) + 1)
 
     right, left = owner(at + 1), owner(at - 1)
+    part_units = w_gate1.shape[1]
+    places = n // 2
+    line, side = fs // 2, fs % 2
+
+    def flip(value, bits):
+        bit = 1
+        while bit <= bits:
+            if bits & bit:
+                value = value + bit - 2 * bit * (value // bit % 2)
+            bit *= 2
+        return value
+
+    def share(place):
+        return (place % 4 + 1) // 2 % 2
+
+    mate = flip(line, 1) * 2 + side
     half = block // 2
     plan = [
         (first_gate, w_gate1, 0, block),
@@ -154,11 +191,13 @@
             device_id_type=MESH,
         )
 
+    @scoped
     def launch(*ks):
         for k in ks:
             for way in (0, 1):
                 ring_copy(k, way, 0).start()
 
+    @scoped
     def serve(k, step):
         for way in (0, 1):
             ring_copy(k, way, step - 1, arriving=True).wait_recv()
@@ -166,21 +205,35 @@
                 ring_copy(k, way, step).start()
 
     barrier = pltpu.get_barrier_semaphore()
-    for target in (left, right):
-        pl.semaphore_signal(barrier, inc=1, device_id={"fs": target}, device_id_type=MESH)
+    for hop in range(1, n):
+        pl.semaphore_signal(
+            barrier, inc=1, device_id={"fs": lax.rem(fs + hop, n)}, device_id_type=MESH
+        )
     for hop in range(1, m):
         pl.semaphore_signal(
             barrier, inc=1, device_id={"tp": lax.rem(tp + hop, m)}, device_id_type=MESH
         )
-    pl.semaphore_wait(barrier, 2 + m - 1)
+    pl.semaphore_wait(barrier, n - 1 + m - 1)
 
     def columns(index, size):
         return pl.ds(pl.multiple_of(index * size, 128), size)
 
+    def full_of(phase):
+        return gathered_mate if phase == 3 else gathered
+
+    def terms_ref(phase):
+        return normed_mate if phase == 3 else normed
+
+    def near_of(phase):
+        return near_mate if phase == 3 else near
+
+    def far_of(phase):
+        return far_mate if phase == 3 else far
+
     def gather_far(phase, hop, source):
         return pltpu.make_async_remote_copy(
             src_ref=source,
-            dst_ref=gathered.at[:, columns(tp, width)],
+            dst_ref=full_of(phase).at[:, columns(tp, width)],
             send_sem=ag_far_send.at[phase, hop],
             recv_sem=ag_far_recv.at[phase, hop],
             device_id={"tp": lax.rem(tp + 2 * hop, m)},
@@ -189,7 +242,7 @@
 
     def gather_near(phase, hop, source=None, arriving=False):
         origin = lax.rem((partner if arriving else tp) - 2 * hop + 2 * m, m)
-        place = gathered.at[:, columns(origin, width)]
+        place = full_of(phase).at[:, columns(origin, width)]
         return pltpu.make_async_remote_copy(
             src_ref=place if source is None else source,
             dst_ref=place,
@@ -201,7 +254,7 @@
 
     def gather_arrived_far(phase, hop):
         origin = lax.rem(tp - 2 * hop + 2 * m, m)
-        place = gathered.at[:, columns(origin, width)]
+        place = full_of(phase).at[:, columns(origin, width)]
         return pltpu.make_async_remote_copy(
             src_ref=place,
             dst_ref=place,
@@ -211,16 +264,19 @@
             device_id_type=MESH,
         )
 
+    @scoped
     def gather_start(phase, source):
         for hop in range(1, chips):
             gather_far(phase, hop, source).start()
         gather_near(phase, 0, source).start()
 
+    @scoped
     def gather_forward(phase):
         for hop in range(1, chips):
             gather_arrived_far(phase, hop).wait_recv()
             gather_near(phase, hop).start()
 
+    @scoped
     def gather_finish(phase, source):
         for hop in range(chips):
             gather_near(phase, hop, arriving=True).wait_recv()
@@ -228,36 +284,55 @@
         for hop in range(1, chips):
             gather_far(phase, hop, source).wait_send()
 
-    def normalise(gain):
+    @scoped
+    def normalise(gain, phase=0):
         size = tile_of(rows, 64)
 
         @pl.loop(0, rows // size)
         def _(i):
             place = pl.ds(pl.multiple_of(i * size, size), size)
-            values = gathered[place, :].astype(F32)
+            values = full_of(phase)[place, :].astype(F32)
             scale = lax.rsqrt(jnp.mean(values * values, axis=-1, keepdims=True) + norm_eps)
-            normed[place, :] = (values * scale * gain[...]).astype(BF16)
+            terms_ref(phase)[place, :] = (values * scale * gain[...]).astype(BF16)
 
     row_tile = tile_of(rows, 256)
-    unit_tile = tile_of(units, 256, 128)
-
-    def hidden_part(gate, up, part, parts):
-        count = rows // row_tile * (units // unit_tile) // parts
-        across = units // unit_tile
+
+    def hidden_view(size):
+        return hidden if size == hidden.shape[1] else hidden_half
+
+    @scoped
+    def hidden_part(gate, up, part, parts, phase=2):
+        size = gate.shape[1]
+        unit_tile = tile_of(size, 256, 640, 128)
+        across = size // unit_tile
+        count = rows // row_tile * across // parts
+        first = rows if phase == 3 else 0
+        source = terms_ref(phase)
+        goal = hidden_view(size)
 
         @pl.loop(part * count, (part + 1) * count)
         def _(i):
-            place = pl.ds(pl.multiple_of((i // across) * row_tile, row_tile), row_tile)
+            start = pl.multiple_of((i // across) * row_tile, row_tile)
+            place = pl.ds(start, row_tile)
             cols = columns(i % across, unit_tile)
-            gate_value = dot(normed[place, :], gate[:, cols])
-            up_value = dot(normed[place, :], up[:, cols])
-            hidden[place, cols] = (jax.nn.silu(gate_value) * up_value).astype(BF16)
+            gate_value = dot(source[place, :], gate[:, cols])
+            up_value = dot(source[place, :], up[:, cols])
+            goal[pl.ds(start + first, row_tile), cols] = (
+                jax.nn.silu(gate_value) * up_value
+            ).astype(BF16)
+
+    def grain(phase):
+        return half if phase == 2 and half % 128 == 0 else block
+
+    def pieces(phase):
+        return width // grain(phase)
 
     def near_copy(phase, b):
+        q, block = pieces(phase), grain(phase)
         slot = b // q // 2 * q + b % q
         return pltpu.make_async_remote_copy(
-            src_ref=terms.at[:, columns(b, block)],
-            dst_ref=near.at[:, columns(slot, block)],
+            src_ref=terms_ref(phase).at[:, columns(b, block)],
+            dst_ref=near_of(phase).at[:, columns(slot, block)],
             send_sem=rs_near_send.at[phase, b],
             recv_sem=rs_near_recv.at[phase, slot],
             device_id={"tp": partner},
@@ -265,32 +340,40 @@
         )
 
     def far_copy(phase, b):
+        q, block = pieces(phase), grain(phase)
         to_chip = b // q // 2
         hop = lax.rem(to_chip - chip + chips, chips)
         slot = (hop - 1) * q + b % q
         return pltpu.make_async_remote_copy(
-            src_ref=terms.at[:, columns(b, block)],
-            dst_ref=far.at[:, columns(slot, block)],
+            src_ref=terms_ref(phase).at[:, columns(b, block)],
+            dst_ref=far_of(phase).at[:, columns(slot, block)],
             send_sem=rs_far_send.at[phase, b],
             recv_sem=rs_far_recv.at[phase, slot],
             device_id={"tp": to_chip * 2 + core},
             device_id_type=MESH,
         )
 
+    @scoped
     def terms_of(phase, left_ref, weight, b):
+        q, block = pieces(phase), grain(phase)
+        first = rows if phase == 3 else 0
+        tall = tile_of(rows, 512)
         weights = pl.ds(pl.multiple_of(b * block, block), block)
 
-        @pl.loop(0, rows // row_tile)
+        @pl.loop(0, rows // tall)
         def _(i):
-            place = pl.ds(pl.multiple_of(i * row_tile, row_tile), row_tile)
-            value = dot_last(left_ref[place, :], weight[weights, :])
-            terms[place, columns(b, block)] = value.astype(BF16)
+            place = pl.ds(pl.multiple_of(i * tall, tall), tall)
+            inner = pl.ds(pl.multiple_of(i * tall + first, tall), tall)
+            value = dot_last(left_ref[inner, :], weight[weights, :])
+            terms_ref(phase)[place, columns(b, block)] = value.astype(BF16)
 
         @pl.when(b // q % 2 != core)
         def _():
             near_copy(phase, b).start()
 
+    @scoped
     def pass_on(phase, b):
+        q, block = pieces(phase), grain(phase)
         mine = b // q % 2 == core
         slot = b // q // 2 * q + b % q
 
@@ -303,9 +386,9 @@
             @pl.loop(0, rows // row_tile)
             def _(i):
                 place = pl.ds(pl.multiple_of(i * row_tile, row_tile), row_tile)
-                total = terms[place, columns(b, block)].astype(F32)
-                total = total + near[place, columns(slot, block)].astype(F32)
-                terms[place, columns(b, block)] = total.astype(BF16)
+                total = terms_ref(phase)[place, columns(b, block)].astype(F32)
+                total = total + near_of(phase)[place, columns(slot, block)].astype(F32)
+                terms_ref(phase)[place, columns(b, block)] = total.astype(BF16)
 
             far_copy(phase, b).start()
 
@@ -317,8 +400,9 @@
         return [owner(at - step), owner(at + step)]
 
     def far_arrived(phase, hop, k):
+        q, block = pieces(phase), grain(phase)
         slot = (hop - 1) * q + k
-        place = far.at[:, slot * block : (slot + 1) * block]
+        place = far_of(phase).at[:, slot * block : (slot + 1) * block]
         return pltpu.make_async_remote_copy(
             src_ref=place,
             dst_ref=place,
@@ -328,25 +412,61 @@
             device_id_type=MESH,
         )
 
-    def finish_sum(phase, factor, whole):
+    def sum_of(phase, place):
+        total = terms_ref(phase)[place, columns(tp, width)].astype(F32)
+        total = total + near_of(phase)[place, columns(chip, width)].astype(F32)
         for hop in range(1, chips):
-            for k in range(q):
-                far_arrived(phase, hop, k).wait_recv()
+            total = total + far_of(phase)[place, (hop - 1) * width : hop * width].astype(F32)
+        return total
+
+    def mate_copy(which):
+        cols = columns(tp, width)
+        return pltpu.make_async_remote_copy(
+            src_ref=normed_mate.at[:, cols] if which else tokens,
+            dst_ref=from_mate if which else gathered_mate.at[:, cols],
+            send_sem=mate_send.at[which],
+            recv_sem=mate_recv.at[which],
+            device_id={"fs": mate},
+            device_id_type=MESH,
+        )
+
+    @scoped
+    def finish_mate():
+        for hop in range(1, chips):
+            for k in range(pieces(3)):
+                far_arrived(3, hop, k).wait_recv()
 
         @pl.loop(0, rows // row_tile)
         def _(i):
             place = pl.ds(pl.multiple_of(i * row_tile, row_tile), row_tile)
-            total = terms[place, columns(tp, width)].astype(F32)
-            total = total + near[place, columns(chip, width)].astype(F32)
-            for hop in range(1, chips):
-                total = total + far[place, (hop - 1) * width : hop * width].astype(F32)
+            normed_mate[place, columns(tp, width)] = sum_of(3, place).astype(BF16)
+
+        mate_copy(1).start()
+
+    @scoped
+    def finish_sum(phase, factor, whole):
+        for hop in range(1, chips):
+            for k in range(pieces(phase)):
+                far_arrived(phase, hop, k).wait_recv()
+        if phase == 0 and split:
+            mate_copy(1).wait_recv()
+            launch(G2, U2)
+
+        @pl.loop(0, rows // row_tile)
+        def _(i):
+            place = pl.ds(pl.multiple_of(i * row_tile, row_tile), row_tile)
+            total = sum_of(phase, place)
+            if phase == 0 and split:
+                total = total + from_mate[place, :].astype(F32)
             value = (stream[place, :].astype(F32) + factor * total).astype(BF16)
             stream[place, :] = value
             if whole:
                 gathered[place, columns(tp, width)] = value
 
+    @scoped
     def sent_sum(phase):
-        for b in range(n):
+        q = pieces(phase)
+        for b in range(q * m):
 
             @pl.when(b // q % 2 != core)
             def _():
@@ -356,8 +476,72 @@
             def _():
                 far_copy(phase, b).wait_send()
 
+    def part_rows(place, beside, low):
+        return pl.ds(pl.multiple_of((place * 2 + beside) * block + low, 16), half)
+
+    def own_part(k, place):
+        low = k % 2 * half
+        return plan[k // 2][0].at[low : low + half, columns(share(place), part_units)]
+
+    def spread_copy(k, bits):
+        other = flip(line, bits)
+        return pltpu.make_async_remote_copy(
+            src_ref=own_part(k, other),
+            dst_ref=plan[k // 2][1].at[part_rows(line, side, k % 2 * half)],
+            send_sem=spread_send.at[k, bits],
+            recv_sem=spread_recv.at[k, bits],
+            device_id={"fs": other * 2 + side},
+            device_id_type=MESH,
+        )
+
+    def spread_arrived(k, bits):
+        place = plan[k // 2][1].at[part_rows(flip(line, bits), side, k % 2 * half)]
+        return pltpu.make_async_remote_copy(
+            src_ref=place,
+            dst_ref=place,
+            send_sem=spread_send.at[k, bits],
+            recv_sem=spread_recv.at[k, bits],
+            device_id={"fs": mate},
+            device_id_type=MESH,
+        )
+
+    def cross_copy(k, bits, arriving=False):
+        beside = 1 - side if arriving else side
+        place = plan[k // 2][1].at[part_rows(flip(line, bits), beside, k % 2 * half)]
+        return pltpu.make_async_remote_copy(
+            src_ref=own_part(k, line) if bits == 0 and not arriving else place,
+            dst_ref=place,
+            send_sem=cross_send.at[k, bits],
+            recv_sem=cross_recv.at[k, bits],
+            device_id={"fs": fs + 1 - 2 * side},
+            device_id_type=MESH,
+        )
+
+    last_first = [*range(2, places), 1]
+
+    @scoped
+    def cross(k):
+        for bits in last_first:
+            spread_arrived(k, bits).wait_recv()
+            cross_copy(k, bits).start()
+            spread_copy(k, bits).wait_send()
+            if k + 2 < 6:
+                spread_copy(k + 2, bits).start()
+
+    @scoped
+    def crossed(k):
+        for part in (2 * k, 2 * k + 1):
+            for bits in range(places):
+                cross_copy(part, bits, arriving=True).wait_recv()
+
+    if split:
+        for bits in range(1, places):
+            spread_copy(0, bits).start()
+        for k in range(6):
+            cross_copy(k, 0).start()
+    else:
+        launch(G1, U1)
     gather_start(0, tokens)
-    launch(G1, U1)
     own = [
         pltpu.make_async_copy(tokens, stream, own_sem.at[0]),
         pltpu.make_async_copy(tokens, gathered.at[:, columns(tp, width)], own_sem.at[1]),
@@ -365,6 +549,8 @@
     mine = pl.ds(pl.multiple_of(fs * block, block), block)
     for k in range(9):
         source, buffer, _, _ = plan[k]
+        if split and k in (G1, U1, D1):
+            source = source.at[:, columns(share(line), part_units)]
         own.append(pltpu.make_async_copy(source, buffer.at[mine], own_sem.at[2 + k]))
     for copy in own:
         copy.start()
@@ -375,38 +561,92 @@
         rate_map[part, part] = rate_weight[k]
         input_map[part, part] = input_weight[k]
     lane[0:8, :] = jnp.zeros((8, lanes), F32)
-    for copy in own:
-        copy.wait()
-
-    serve(G1, 1)
-    gather_forward(0)
-    serve(U1, 1)
-    gather_finish(0, tokens)
-    normalise(first_gain)
-    for step in range(2, h + 1):
-        serve(G1, step)
-        serve(U1, step)
-        if step == h - 1:
-            launch(D1)
-    launch(MI, MB, MO)
-    hidden_part(w_gate1, w_up1, 0, 1)
-    for b in blocks_at(0):
-        terms_of(0, hidden, w_down1, b)
-    for step in range(1, h + 1):
-        serve(D1, step)
-        for b in blocks_at(step):
+    with jax.named_scope("ownwait"):
+        for copy in own:
+            copy.wait()
+
+    if split:
+        own_cols = gathered_mate.at[:, columns(tp, width)]
+        mixes = [(k, step) for step in range(1, h + 1) for k in (MI, MB, MO)]
+
+        def mix_serve(count):
+            for _ in range(min(count, len(mixes))):
+                serve(*mixes.pop(0))
+
+        for bits in range(1, places):
+            spread_copy(1, bits).start()
+        cross(0)
+        mate_copy(0).start()
+        gather_forward(0)
+        cross(1)
+        gather_finish(0, tokens)
+        normalise(first_gain)
+        cross(2)
+        with jax.named_scope("matewait"):
+            mate_copy(0).wait_recv()
+        gather_start(3, own_cols)
+        cross(3)
+        cross(4)
+        gather_forward(3)
+        cross(5)
+        gather_finish(3, own_cols)
+        normalise(first_gain, 3)
+        crossed(G1)
+        crossed(U1)
+        parts = tile_of(rows // row_tile, 4, 2)
+        launch(MI, MB, MO)
+        hidden_part(w_gate1, w_up1, 0, 1, 3)
+        crossed(D1)
+        for b in range(n):
+            terms_of(3, hidden_half, w_down1, b)
+            if b:
+                pass_on(3, b - 1)
+        pass_on(3, n - 1)
+        mix_serve(3)
+        for part in range(parts):
+            hidden_part(w_gate1, w_up1, part, parts, 0)
+            if part == 1:
+                mix_serve(3)
+        mix_serve(3)
+        finish_mate()
+        mix_serve(len(mixes))
+        for b in range(n):
+            terms_of(0, hidden_half, w_down1, b)
+            if b:
+                pass_on(0, b - 1)
+        pass_on(0, n - 1)
+    else:
+        serve(G1, 1)
+        gather_forward(0)
+        serve(U1, 1)
+        gather_finish(0, tokens)
+        normalise(first_gain)
+        for step in range(2, h + 1):
+            serve(G1, step)
+            serve(U1, step)
+            if step == h - 1:
+                launch(D1)
+        launch(MI, MB, MO)
+        hidden_part(w_gate1, w_up1, 0, 1, 0)
+        for b in blocks_at(0):
             terms_of(0, hidden, w_down1, b)
-        for k in (MI, MB, MO):
-            serve(k, step)
-        for b in blocks_at(step - 1):
+        for step in range(1, h + 1):
+            serve(D1, step)
+            for b in blocks_at(step):
+                terms_of(0, hidden, w_down1, b)
+            for k in (MI, MB, MO):
+                serve(k, step)
+            for b in blocks_at(step - 1):
+                pass_on(0, b)
+            if step == h - 1:
+                launch(G2, U2)
+        for b in blocks_at(h):
             pass_on(0, b)
-        if step == h - 1:
-            launch(G2, U2)
-    for b in blocks_at(h):
-        pass_on(0, b)
     finish_sum(0, 0.5, True)
     gather_start(1, stream)
     sent_sum(0)
+    if split:
+        sent_sum(3)
 
     queue = [(k, step) for step in range(1, h + 1) for k in (G2, U2)]
 
@@ -419,7 +659,6 @@
 
     take(1)
     gather_forward(1)
-    take(1)
     gather_finish(1, stream)
     normalise(mix_gain)
 
@@ -433,7 +672,6 @@
 
     slope = -rate_scale * jnp.log1p(jnp.exp(-decay_param[...]))
     small = tile_of(rows, 128)
-    lane_id = lax.broadcasted_iota(jnp.int32, (small, lanes), 1) // HEAD_DIM
 
     @pl.loop(0, rows // small)
     def _(i):
@@ -446,17 +684,20 @@
         conv_out = conv_sum.astype(BF16)
         rate = jax.nn.sigmoid(dot(conv_out, rate_map[...]))
         admit = jax.nn.sigmoid(dot(conv_out, input_map[...]))
-        shifts = decay_shift[place, :]
-        shift = jnp.zeros((small, lanes), F32)
-        for k in range(lanes // HEAD_DIM):
-            shift = jnp.where(lane_id == k, shifts[:, k : k + 1], shift)
+        shifts = decay_shift[:, columns(i, small)]
+        shift = jnp.concatenate(
+            [
+                jnp.broadcast_to(shifts[k : k + 1, :], (HEAD_DIM, small))
+                for k in range(lanes // HEAD_DIM)
+            ],
+            axis=0,
+        ).T
         log_decay = rate * slope + shift
         decay[place, :] = jnp.exp(log_decay)
         drive[place, :] = (
             jnp.sqrt(negative_expm1(2.0 * log_decay)) * admit * conv_out.astype(F32)
         )
 
-    take(1)
     lane_tile = tile_of(lanes, 128)
     row_id = lax.broadcasted_iota(jnp.int32, (rows, lane_tile), 0)
 
@@ -474,40 +715,42 @@
         mixed[:, cols] = (state * jax.nn.gelu(branch[:, cols])).astype(BF16)
 
     take(1)
-    for step in range(h + 1):
-        for b in blocks_at(step):
-            terms_of(1, mixed, w_out, b)
-        if step:
-            for b in blocks_at(step - 1):
-                pass_on(1, b)
-    for b in blocks_at(h):
-        pass_on(1, b)
+    for b in range(n):
+        terms_of(1, mixed, w_out, b)
+        if b:
+            pass_on(1, b - 1)
+    pass_on(1, n - 1)
     take(1)
     finish_sum(1, 1.0, True)
     gather_start(2, stream)
     sent_sum(1)
-    take(1)
+    take(3)
     gather_forward(2)
+    take(2 * h - 1 - 6)
+    gather_finish(2, stream)
+    normalise(second_gain)
     take(2 * h)
-    gather_finish(2, stream)
-
-    normalise(second_gain)
+
     halves = [(k, step) for step in range(1, h + 1) for k in (D2A, D2B)]
     parts = tile_of(rows // row_tile, 4, 2)
     for part in range(parts):
-        serve(*halves.pop(0))
         hidden_part(w_gate2, w_up2, part, parts)
-    for b in blocks_at(0):
-        terms_of(2, hidden, w_down2, b)
-    for step in range(1, h + 1):
-        while halves and halves[0][1] <= step:
+        if part % 2 or parts < 4:
             serve(*halves.pop(0))
-        for b in blocks_at(step):
-            terms_of(2, hidden, w_down2, b)
-        for b in blocks_at(step - 1):
-            pass_on(2, b)
-    for b in blocks_at(h):
-        pass_on(2, b)
+    fine = block // grain(2)
+    for step in range(h + 1):
+        for piece in range(2):
+            while halves and (halves[0][1], halves[0][0]) <= (step, D2A + piece):
+                serve(*halves.pop(0))
+            if fine == 1 and piece == 0:
+                continue
+            fresh = [
+                b * fine + e for b in blocks_at(step) for e in ([piece] if fine == 2 else [0])
+            ]
+            for b in fresh:
+                terms_of(2, hidden, w_down2, b)
+            for b in fresh:
+                pass_on(2, b)
     finish_sum(2, 0.5, False)
 
     @pl.loop(0, rows // row_tile)
@@ -530,12 +773,19 @@
     for hop in range(1, m):
         square_copy(hop).start()
     sent_sum(2)
-    for k in range(len(plan)):
+    for k in range(MI if split else 0, len(plan)):
         for way in (0, 1):
             for step in range(h):
                 ring_copy(k, way, step).wait_send()
-    for hop in range(1, m):
-        square_copy(hop).wait()
+    if split:
+        for k in range(6):
+            for bits in range(places):
+                cross_copy(k, bits).wait_send()
+        for which in range(2):
+            mate_copy(which).wait_send()
+    with jax.named_scope("sqwait"):
+        for hop in range(1, m):
+            square_copy(hop).wait()
 
     @pl.loop(0, rows // row_tile)
     def _(i):
@@ -545,7 +795,8 @@
         for hop in range(1, m):
             squares = squares + square_in[hop - 1, :, cols]
         spread = jnp.broadcast_to(squares[0:1, :], (128, row_tile)).T
-        scale_out[place, :] = lax.rsqrt(spread / d + norm_eps)
+        scale = lax.rsqrt(spread[:, 0:1] / d + norm_eps)
+        stream[place, :] = (stream[place, :].astype(F32) * scale * final_gain[...]).astype(BF16)
 
 
 def shards(n, m, *arrays):
@@ -575,27 +826,32 @@
     units = first_gate.shape[1]
     lanes = mix_input.shape[1]
     h, q, chips = n // 2, n // m, m // 2
+    split = units % 256 == 0 and h % 4 == 0 and h & (h - 1) == 0
+    part_units = units // 2 if split else units
     hbm = pl.BlockSpec(memory_space=pl.ANY)
     vmem = pl.BlockSpec(memory_space=pltpu.VMEM)
     dma = pltpu.SemaphoreType.DMA
-    stream, scale = pl.pallas_call(
-        functools.partial(kernel, n, m),
-        out_shape=(
-            jax.ShapeDtypeStruct((rows, width), BF16),
-            jax.ShapeDtypeStruct((rows, 128), F32),
-        ),
-        in_specs=[hbm] * 10 + [vmem] * 8,
-        out_specs=(vmem, vmem),
+    spare = pltpu.VMEM((16, 128), BF16)
+    return pl.pallas_call(
+        functools.partial(kernel, n, m, split),
+        out_shape=jax.ShapeDtypeStruct((rows, width), BF16),
+        in_specs=[hbm] * 10 + [vmem] * 9,
+        out_specs=vmem,
         scratch_shapes=[
-            *[pltpu.VMEM((d, units), BF16)] * 3,
+            *[pltpu.VMEM((d, part_units), BF16)] * 3,
             *[pltpu.VMEM((d, lanes), BF16)] * 3,
             *[pltpu.VMEM((d, units), BF16)] * 3,
             pltpu.VMEM((rows, d), BF16),
+            pltpu.VMEM((rows, d), BF16) if split else spare,
             pltpu.VMEM((rows, d), BF16),
+            pltpu.VMEM((rows, d), BF16) if split else spare,
             pltpu.VMEM((rows, units), BF16),
-            pltpu.VMEM((rows, d), BF16),
+            pltpu.VMEM((2 * rows, part_units), BF16) if split else spare,
             pltpu.VMEM((rows, chips * width), BF16),
+            pltpu.VMEM((rows, chips * width), BF16) if split else spare,
             pltpu.VMEM((rows, max(chips - 1, 1) * width), BF16),
+            pltpu.VMEM((rows, max(chips - 1, 1) * width), BF16) if split else spare,
+            pltpu.VMEM((rows, width), BF16) if split else spare,
             pltpu.VMEM((rows, lanes), BF16),
             pltpu.VMEM((rows + 8, lanes), F32),
             pltpu.VMEM((rows, lanes), F32),
@@ -608,16 +864,22 @@
             dma((10, 2, h)),
             dma((10, 2, h)),
             dma((11,)),
-            dma((3, chips)),
-            dma((3, chips)),
-            dma((3, chips)),
-            dma((3, chips)),
-            dma((3, n)),
-            dma((3, n // 2)),
-            dma((3, n)),
-            dma((3, max(chips - 1, 1) * q)),
+            dma((4, chips)),
+            dma((4, chips)),
+            dma((4, chips)),
+            dma((4, chips)),
+            dma((4, 2 * n)),
+            dma((4, n)),
+            dma((4, 2 * n)),
+            dma((4, max(chips - 1, 1) * q * 2)),
             dma((m,)),
             dma((m,)),
+            dma((6, h)),
+            dma((6, h)),
+            dma((6, h)),
+            dma((6, h)),
+            dma((2,)),
+            dma((2,)),
         ],
         compiler_params=pltpu.CompilerParams(
             collective_id=0, has_side_effects=True, vmem_limit_bytes=67043328
@@ -643,9 +905,9 @@
         rate_weight,
         input_weight,
         decay_param[None, :],
-        decay_shift,
+        decay_shift.T,
+        final_gain[None, :],
     )
-    return (stream.astype(F32) * scale[:, :1] * final_gain).astype(BF16)
 
 
 def solution(mesh):

time: 376 us -> 347 us (0.923)
  Pallas kernels: 370 us -> 345 us
    pallas_call x1, Pallas kernels: 370 us -> 345 us  [shards(): pl.pallas_call(functools.partial(kernel, n, m, split), out_shape=jax.Shap...]
where the time goes in v1:
time: 347 us
  Pallas kernels  345 us (99%)
    pallas_call x1, Pallas kernels, shards(): pl.pallas_call(functools.partial(kernel, n, m, split), out_shape=jax.Shap...  345 us

profile of v1, /device:TPU:0, one launch (start us, length us, event | category | flops | bytes accessed | tf_op | source)
XLA Modules:
  0.0 346.8 jit_solution(14085240081716168640)
XLA Ops:
  0.0 344.5 %shard_map.181 = bf16[1024,512]{1,0:T(8,128)(2,1)} custom-call(bf16[1024,512]{1,0:T(8,128)(2,1)} %tokens.1, bf16[256,1280]{1,0:T(8,128)(2,1)} %first_gate.1, bf16[256,1280]{1,0:T(8,128)(2,1)} %first_up.1, bf16[256,1280]{1,0:T(8,128)(2,1)} %first_down.1, bf16[256,256]{1,0:T(8,128)(2,1)} %mix_input.1, bf16[256,256]{1,0:T(8,128)(2,1)} %mix_branch.1, ...), custom_call_target="tpu_custom_call" | custom-call | flops 35433480192 | bytes 20971520 | tf_op jit(solution)/shard_map/pallas_call | solution.py:835
  344.5 2.3 copy.21

commit v2 on v1

--- a/solution.py
+++ b/solution.py
@@ -70,6 +70,7 @@
     decay_param,
     decay_shift,
     final_gain,
+    out,
     stream,
     w_gate1,
     w_up1,
@@ -170,6 +171,8 @@
         (second_down, w_down2, half, half),
     ]
 
+    ring_low = G2 if split else 0
+
     def ring_copy(k, way, step, arriving=False):
         source, buffer, low, count = plan[k]
         sign = -1 if way == 0 else 1
@@ -185,8 +188,8 @@
         return pltpu.make_async_remote_copy(
             src_ref=src,
             dst_ref=buffer.at[place],
-            send_sem=ring_send.at[k, way, step],
-            recv_sem=ring_recv.at[k, way, step],
+            send_sem=ring_send.at[k - ring_low, way, step],
+            recv_sem=ring_recv.at[k - ring_low, way, step],
             device_id={"fs": right if way == 0 else left},
             device_id_type=MESH,
         )
@@ -333,7 +336,7 @@
         return pltpu.make_async_remote_copy(
             src_ref=terms_ref(phase).at[:, columns(b, block)],
             dst_ref=near_of(phase).at[:, columns(slot, block)],
-            send_sem=rs_near_send.at[phase, b],
+            send_sem=rs_near_send.at[phase // 3, b],
             recv_sem=rs_near_recv.at[phase, slot],
             device_id={"tp": partner},
             device_id_type=MESH,
@@ -347,7 +350,7 @@
         return pltpu.make_async_remote_copy(
             src_ref=terms_ref(phase).at[:, columns(b, block)],
             dst_ref=far_of(phase).at[:, columns(slot, block)],
-            send_sem=rs_far_send.at[phase, b],
+            send_sem=rs_far_send.at[phase // 3, b],
             recv_sem=rs_far_recv.at[phase, slot],
             device_id={"tp": to_chip * 2 + core},
             device_id_type=MESH,
@@ -392,6 +395,9 @@
 
             far_copy(phase, b).start()
 
+    def turn(b):
+        return lax.rem(b + (chip + 1) * (n // chips), n)
+
     def blocks_at(step):
         if step == 0:
             return [fs]
@@ -406,7 +412,7 @@
         return pltpu.make_async_remote_copy(
             src_ref=place,
             dst_ref=place,
-            send_sem=rs_far_send.at[phase, 0],
+            send_sem=rs_far_send.at[phase // 3, 0],
             recv_sem=rs_far_recv.at[phase, slot],
             device_id={"tp": partner},
             device_id_type=MESH,
@@ -419,16 +425,28 @@
             total = total + far_of(phase)[place, (hop - 1) * width : hop * width].astype(F32)
         return total
 
-    def mate_copy(which):
+    chunks = 1
+    chunk = rows // chunks
+
+    def mate_copy(which, c):
         cols = columns(tp, width)
-        return pltpu.make_async_remote_copy(
-            src_ref=normed_mate.at[:, cols] if which else tokens,
-            dst_ref=from_mate if which else gathered_mate.at[:, cols],
-            send_sem=mate_send.at[which],
-            recv_sem=mate_recv.at[which],
+        part = pl.ds(c * chunk, chunk)
+        return pltpu.make_async_remote_copy(
+            src_ref=normed_mate.at[part, cols] if which else tokens.at[part],
+            dst_ref=from_mate.at[part] if which else gathered_mate.at[part, cols],
+            send_sem=mate_send.at[which, c],
+            recv_sem=mate_recv.at[which, c],
             device_id={"fs": mate},
             device_id_type=MESH,
         )
+
+    def mate_start(which):
+        for c in range(chunks):
+            mate_copy(which, c).start()
+
+    def mate_arrived(which):
+        for c in range(chunks):
+            mate_copy(which, c).wait_recv()
 
     @scoped
     def finish_mate():
@@ -441,7 +459,7 @@
             place = pl.ds(pl.multiple_of(i * row_tile, row_tile), row_tile)
             normed_mate[place, columns(tp, width)] = sum_of(3, place).astype(BF16)
 
-        mate_copy(1).start()
+        mate_start(1)
 
     @scoped
     def finish_sum(phase, factor, whole):
@@ -449,8 +467,8 @@
             for k in range(pieces(phase)):
                 far_arrived(phase, hop, k).wait_recv()
         if phase == 0 and split:
-            mate_copy(1).wait_recv()
-            launch(G2, U2)
+            mate_arrived(1)
+            launch(U2)
 
         @pl.loop(0, rows // row_tile)
         def _(i):
@@ -476,30 +494,38 @@
             def _():
                 far_copy(phase, b).wait_send()
 
-    def part_rows(place, beside, low):
-        return pl.ds(pl.multiple_of((place * 2 + beside) * block + low, 16), half)
+    def piece_of(k):
+        if k < 6:
+            return (*plan[k // 2][:2], k % 2 * half, half)
+        return plan[k - 3]
+
+    def part_rows(k, place, beside):
+        low, count = piece_of(k)[2:]
+        return pl.ds(pl.multiple_of((place * 2 + beside) * block + low, 16), count)
 
     def own_part(k, place):
-        low = k % 2 * half
-        return plan[k // 2][0].at[low : low + half, columns(share(place), part_units)]
+        source, _, low, count = piece_of(k)
+        if k >= 6:
+            return source
+        return source.at[low : low + count, columns(share(place), part_units)]
 
     def spread_copy(k, bits):
         other = flip(line, bits)
         return pltpu.make_async_remote_copy(
             src_ref=own_part(k, other),
-            dst_ref=plan[k // 2][1].at[part_rows(line, side, k % 2 * half)],
-            send_sem=spread_send.at[k, bits],
+            dst_ref=piece_of(k)[1].at[part_rows(k, line, side)],
+            send_sem=spread_send.at[k % 3, bits],
             recv_sem=spread_recv.at[k, bits],
             device_id={"fs": other * 2 + side},
             device_id_type=MESH,
         )
 
     def spread_arrived(k, bits):
-        place = plan[k // 2][1].at[part_rows(flip(line, bits), side, k % 2 * half)]
+        place = piece_of(k)[1].at[part_rows(k, flip(line, bits), side)]
         return pltpu.make_async_remote_copy(
             src_ref=place,
             dst_ref=place,
-            send_sem=spread_send.at[k, bits],
+            send_sem=spread_send.at[k % 3, bits],
             recv_sem=spread_recv.at[k, bits],
             device_id={"fs": mate},
             device_id_type=MESH,
@@ -507,7 +533,7 @@
 
     def cross_copy(k, bits, arriving=False):
         beside = 1 - side if arriving else side
-        place = plan[k // 2][1].at[part_rows(flip(line, bits), beside, k % 2 * half)]
+        place = piece_of(k)[1].at[part_rows(k, flip(line, bits), beside)]
         return pltpu.make_async_remote_copy(
             src_ref=own_part(k, line) if bits == 0 and not arriving else place,
             dst_ref=place,
@@ -517,6 +543,7 @@
             device_id_type=MESH,
         )
 
+    mixes = range(6, 9)
     last_first = [*range(2, places), 1]
 
     @scoped
@@ -529,8 +556,8 @@
                 spread_copy(k + 2, bits).start()
 
     @scoped
-    def crossed(k):
-        for part in (2 * k, 2 * k + 1):
+    def crossed(*parts):
+        for part in parts:
             for bits in range(places):
                 cross_copy(part, bits, arriving=True).wait_recv()
 
@@ -567,54 +594,48 @@
 
     if split:
         own_cols = gathered_mate.at[:, columns(tp, width)]
-        mixes = [(k, step) for step in range(1, h + 1) for k in (MI, MB, MO)]
-
-        def mix_serve(count):
-            for _ in range(min(count, len(mixes))):
-                serve(*mixes.pop(0))
-
         for bits in range(1, places):
             spread_copy(1, bits).start()
         cross(0)
-        mate_copy(0).start()
+        mate_start(0)
         gather_forward(0)
         cross(1)
         gather_finish(0, tokens)
         normalise(first_gain)
         cross(2)
         with jax.named_scope("matewait"):
-            mate_copy(0).wait_recv()
+            mate_arrived(0)
         gather_start(3, own_cols)
         cross(3)
         cross(4)
         gather_forward(3)
         cross(5)
+        for k in mixes:
+            for bits in range(1, places):
+                spread_copy(k, bits).start()
         gather_finish(3, own_cols)
         normalise(first_gain, 3)
-        crossed(G1)
-        crossed(U1)
-        parts = tile_of(rows // row_tile, 4, 2)
-        launch(MI, MB, MO)
+        crossed(0, 1, 2, 3)
         hidden_part(w_gate1, w_up1, 0, 1, 3)
-        crossed(D1)
+        crossed(4, 5)
+        launch(G2)
+        for k in mixes:
+            cross_copy(k, 0).start()
         for b in range(n):
-            terms_of(3, hidden_half, w_down1, b)
+            terms_of(3, hidden_half, w_down1, turn(b))
             if b:
-                pass_on(3, b - 1)
-        pass_on(3, n - 1)
-        mix_serve(3)
-        for part in range(parts):
-            hidden_part(w_gate1, w_up1, part, parts, 0)
-            if part == 1:
-                mix_serve(3)
-        mix_serve(3)
-        finish_mate()
-        mix_serve(len(mixes))
+                pass_on(3, turn(b - 1))
+        pass_on(3, turn(n - 1))
+        hidden_part(w_gate1, w_up1, 0, 1, 0)
         for b in range(n):
-            terms_of(0, hidden_half, w_down1, b)
+            terms_of(0, hidden_half, w_down1, turn(b))
             if b:
-                pass_on(0, b - 1)
-        pass_on(0, n - 1)
+                pass_on(0, turn(b - 1))
+            if b == n // 2 - 1:
+                finish_mate()
+        pass_on(0, turn(n - 1))
+        for k in mixes:
+            cross(k)
     else:
         serve(G1, 1)
         gather_forward(0)
@@ -654,13 +675,18 @@
         for _ in range(min(count, len(queue))):
             k, step = queue.pop(0)
             serve(k, step)
-            if k == U2 and step == h - 1:
-                launch(D2A, D2B)
+            if (k, step) == (G2, h):
+                launch(D2A)
+            if (k, step) == (U2, h):
+                launch(D2B)
 
     take(1)
     gather_forward(1)
+    take(1)
     gather_finish(1, stream)
     normalise(mix_gain)
+    if split:
+        crossed(*mixes)
 
     @pl.loop(0, rows // row_tile)
     def _(i):
@@ -670,6 +696,7 @@
         lane[lower, :] = value.astype(BF16).astype(F32)
         branch[place, :] = dot(normed[place, :], w_branch[...])
 
+    take(1)
     slope = -rate_scale * jnp.log1p(jnp.exp(-decay_param[...]))
     small = tile_of(rows, 128)
 
@@ -714,33 +741,36 @@
             reach *= 2
         mixed[:, cols] = (state * jax.nn.gelu(branch[:, cols])).astype(BF16)
 
-    take(1)
     for b in range(n):
-        terms_of(1, mixed, w_out, b)
+        terms_of(1, mixed, w_out, turn(b))
         if b:
-            pass_on(1, b - 1)
-    pass_on(1, n - 1)
-    take(1)
+            pass_on(1, turn(b - 1))
+    pass_on(1, turn(n - 1))
+    take(2)
     finish_sum(1, 1.0, True)
     gather_start(2, stream)
     sent_sum(1)
-    take(3)
+    take(2 * h)
     gather_forward(2)
-    take(2 * h - 1 - 6)
+    halves = [(k, step) for step in range(1, h + 1) for k in (D2A, D2B)]
+    serve(*halves.pop(0))
     gather_finish(2, stream)
     normalise(second_gain)
-    take(2 * h)
-
-    halves = [(k, step) for step in range(1, h + 1) for k in (D2A, D2B)]
+
     parts = tile_of(rows // row_tile, 4, 2)
     for part in range(parts):
         hidden_part(w_gate2, w_up2, part, parts)
-        if part % 2 or parts < 4:
+        if part < 2:
             serve(*halves.pop(0))
     fine = block // grain(2)
     for step in range(h + 1):
         for piece in range(2):
-            while halves and (halves[0][1], halves[0][0]) <= (step, D2A + piece):
+            reach = (step, D2A + piece)
+            if step == 0:
+                reach = (2 * piece, D2B)
+            elif (step, piece) == (1, 1):
+                reach = (3, D2A)
+            while halves and (halves[0][1], halves[0][0]) <= reach:
                 serve(*halves.pop(0))
             if fine == 1 and piece == 0:
                 continue
@@ -773,30 +803,38 @@
     for hop in range(1, m):
         square_copy(hop).start()
     sent_sum(2)
-    for k in range(MI if split else 0, len(plan)):
+    for k in range(G2 if split else 0, len(plan)):
         for way in (0, 1):
             for step in range(h):
                 ring_copy(k, way, step).wait_send()
     if split:
-        for k in range(6):
+        for k in range(9):
             for bits in range(places):
                 cross_copy(k, bits).wait_send()
         for which in range(2):
-            mate_copy(which).wait_send()
+            for c in range(chunks):
+                mate_copy(which, c).wait_send()
     with jax.named_scope("sqwait"):
         for hop in range(1, m):
             square_copy(hop).wait()
 
-    @pl.loop(0, rows // row_tile)
-    def _(i):
-        place = pl.ds(pl.multiple_of(i * row_tile, row_tile), row_tile)
-        cols = columns(i, row_tile)
-        squares = square_own[:, cols]
-        for hop in range(1, m):
-            squares = squares + square_in[hop - 1, :, cols]
-        spread = jnp.broadcast_to(squares[0:1, :], (128, row_tile)).T
-        scale = lax.rsqrt(spread[:, 0:1] / d + norm_eps)
-        stream[place, :] = (stream[place, :].astype(F32) * scale * final_gain[...]).astype(BF16)
+    def out_copy(i):
+        place = pl.ds(i * row_tile, row_tile)
+        return pltpu.make_async_copy(stream.at[place], out.at[place], own_sem.at[i])
+
+    with jax.named_scope("final"):
+        for i in range(rows // row_tile):
+            place = slice(i * row_tile, (i + 1) * row_tile)
+            squares = square_own[:, place]
+            for hop in range(1, m):
+                squares = squares + square_in[hop - 1, :, place]
+            spread = jnp.broadcast_to(squares[0:1, :], (128, row_tile)).T
+            scale = lax.rsqrt(spread[:, 0:1] / d + norm_eps)
+            stream[place, :] = (stream[place, :].astype(F32) * scale * final_gain[...]).astype(BF16)
+            out_copy(i).start()
+    with jax.named_scope("outwait"):
+        for i in range(rows // row_tile):
+            out_copy(i).wait()
 
 
 def shards(n, m, *arrays):
@@ -836,8 +874,9 @@
         functools.partial(kernel, n, m, split),
         out_shape=jax.ShapeDtypeStruct((rows, width), BF16),
         in_specs=[hbm] * 10 + [vmem] * 9,
-        out_specs=vmem,
+        out_specs=hbm,
         scratch_shapes=[
+            pltpu.VMEM((rows, width), BF16),
             *[pltpu.VMEM((d, part_units), BF16)] * 3,
             *[pltpu.VMEM((d, lanes), BF16)] * 3,
             *[pltpu.VMEM((d, units), BF16)] * 3,
@@ -861,25 +900,25 @@
             pltpu.VMEM((lanes, lanes), BF16),
             pltpu.VMEM((8, rows), F32),
             pltpu.VMEM((m - 1, 8, rows), F32),
-            dma((10, 2, h)),
-            dma((10, 2, h)),
+            dma((4 if split else 10, 2, h)),
+            dma((4 if split else 10, 2, h)),
             dma((11,)),
             dma((4, chips)),
             dma((4, chips)),
             dma((4, chips)),
             dma((4, chips)),
-            dma((4, 2 * n)),
+            dma((2, 2 * n)),
             dma((4, n)),
-            dma((4, 2 * n)),
+            dma((2, 2 * n)),
             dma((4, max(chips - 1, 1) * q * 2)),
             dma((m,)),
             dma((m,)),
-            dma((6, h)),
-            dma((6, h)),
-            dma((6, h)),
-            dma((6, h)),
-            dma((2,)),
-            dma((2,)),
+            dma((3, h)),
+            dma((9, h)),
+            dma((9, h)),
+            dma((9, h)),
+            dma((2, 1)),
+            dma((2, 1)),
         ],
         compiler_params=pltpu.CompilerParams(
             collective_id=0, has_side_effects=True, vmem_limit_bytes=67043328

time: 347 us -> 335 us (0.965)
  Pallas kernels: 345 us -> 330 us
    pallas_call x1, Pallas kernels: 345 us -> 330 us  [shards(): pl.pallas_call(functools.partial(kernel, n, m, split), out_shape=jax.Shap...]
where the time goes in v2:
time: 335 us; the launch traced here: 333 us
  Pallas kernels  330 us (99%)
    pallas_call x1, Pallas kernels, shards(): pl.pallas_call(functools.partial(kernel, n, m, split), out_shape=jax.Shap...  330 us

profile of v2, /device:TPU:0, one launch (start us, length us, event | category | flops | bytes accessed | tf_op | source)
XLA Modules:
  0.0 332.8 jit_solution(7346239068105851749)
XLA Ops:
  0.0 330.5 %shard_map.181 = bf16[1024,512]{1,0:T(8,128)(2,1)} custom-call(bf16[1024,512]{1,0:T(8,128)(2,1)} %tokens.1, bf16[256,1280]{1,0:T(8,128)(2,1)} %first_gate.1, bf16[256,1280]{1,0:T(8,128)(2,1)} %first_up.1, bf16[256,1280]{1,0:T(8,128)(2,1)} %first_down.1, bf16[256,256]{1,0:T(8,128)(2,1)} %mix_input.1, bf16[256,256]{1,0:T(8,128)(2,1)} %mix_branch.1, ...), custom_call_target="tpu_custom_call" | custom-call | flops 35433480192 | bytes 20971520 | tf_op jit(solution)/shard_map/pallas_call | solution.py:873
  330.5 2.3 copy.21

commit v3 on v2

--- a/solution.py
+++ b/solution.py
@@ -357,22 +357,24 @@
         )
 
     @scoped
-    def terms_of(phase, left_ref, weight, b):
+    def terms_of(phase, left_ref, weight, b, many=1):
         q, block = pieces(phase), grain(phase)
         first = rows if phase == 3 else 0
         tall = tile_of(rows, 512)
-        weights = pl.ds(pl.multiple_of(b * block, block), block)
+        weights = pl.ds(pl.multiple_of(b * block * many, block), block * many)
 
         @pl.loop(0, rows // tall)
         def _(i):
             place = pl.ds(pl.multiple_of(i * tall, tall), tall)
             inner = pl.ds(pl.multiple_of(i * tall + first, tall), tall)
             value = dot_last(left_ref[inner, :], weight[weights, :])
-            terms_ref(phase)[place, columns(b, block)] = value.astype(BF16)
-
-        @pl.when(b // q % 2 != core)
-        def _():
-            near_copy(phase, b).start()
+            terms_ref(phase)[place, columns(b, block * many)] = value.astype(BF16)
+
+        for e in range(many):
+
+            @pl.when((b * many + e) // q % 2 != core)
+            def _():
+                near_copy(phase, b * many + e).start()
 
     @scoped
     def pass_on(phase, b):
@@ -627,15 +629,24 @@
                 pass_on(3, turn(b - 1))
         pass_on(3, turn(n - 1))
         hidden_part(w_gate1, w_up1, 0, 1, 0)
+
+        @pl.when(core == 0)
+        def _():
+            finish_mate()
+
         for b in range(n):
             terms_of(0, hidden_half, w_down1, turn(b))
             if b:
                 pass_on(0, turn(b - 1))
             if b == n // 2 - 1:
-                finish_mate()
+                for k in mixes:
+                    cross(k)
+
+                @pl.when(core == 1)
+                def _():
+                    finish_mate()
+
         pass_on(0, turn(n - 1))
-        for k in mixes:
-            cross(k)
     else:
         serve(G1, 1)
         gather_forward(0)
@@ -699,6 +710,7 @@
     take(1)
     slope = -rate_scale * jnp.log1p(jnp.exp(-decay_param[...]))
     small = tile_of(rows, 128)
+    lane_id = lax.broadcasted_iota(jnp.int32, (small, lanes), 1) // HEAD_DIM
 
     @pl.loop(0, rows // small)
     def _(i):
@@ -712,13 +724,10 @@
         rate = jax.nn.sigmoid(dot(conv_out, rate_map[...]))
         admit = jax.nn.sigmoid(dot(conv_out, input_map[...]))
         shifts = decay_shift[:, columns(i, small)]
-        shift = jnp.concatenate(
-            [
-                jnp.broadcast_to(shifts[k : k + 1, :], (HEAD_DIM, small))
-                for k in range(lanes // HEAD_DIM)
-            ],
-            axis=0,
-        ).T
+        shifts = jnp.concatenate([shifts] * (8 // shifts.shape[0]), axis=0).T
+        shift = jnp.zeros((small, lanes), F32)
+        for k in range(lanes // HEAD_DIM):
+            shift = jnp.where(lane_id == k, shifts[:, k : k + 1], shift)
         log_decay = rate * slope + shift
         decay[place, :] = jnp.exp(log_decay)
         drive[place, :] = (
@@ -760,18 +769,26 @@
     parts = tile_of(rows // row_tile, 4, 2)
     for part in range(parts):
         hidden_part(w_gate2, w_up2, part, parts)
-        if part < 2:
+        if part != 2:
             serve(*halves.pop(0))
     fine = block // grain(2)
+    held = []
     for step in range(h + 1):
+        if step <= 2:
+            while halves and halves[0][1] <= step:
+                serve(*halves.pop(0))
+            for b in blocks_at(step):
+                terms_of(2, hidden, w_down2, b, fine)
+            for b in held:
+                pass_on(2, b)
+            held = [b * fine + e for b in blocks_at(step) for e in range(fine)]
+            continue
         for piece in range(2):
-            reach = (step, D2A + piece)
-            if step == 0:
-                reach = (2 * piece, D2B)
-            elif (step, piece) == (1, 1):
-                reach = (3, D2A)
-            while halves and (halves[0][1], halves[0][0]) <= reach:
+            while halves and (halves[0][1], halves[0][0]) <= (step, D2A + piece):
                 serve(*halves.pop(0))
+            for b in held:
+                pass_on(2, b)
+            held = []
             if fine == 1 and piece == 0:
                 continue
             fresh = [

time: 335 us -> 323 us (0.964)
  Pallas kernels: 330 us -> 321 us
    pallas_call x1, Pallas kernels: 330 us -> 321 us  [shards(): pl.pallas_call(functools.partial(kernel, n, m, split), out_shape=jax.Shap...]
where the time goes in v3:
time: 323 us
  Pallas kernels  321 us (99%)
    pallas_call x1, Pallas kernels, shards(): pl.pallas_call(functools.partial(kernel, n, m, split), out_shape=jax.Shap...  321 us

profile of v3, /device:TPU:0, one launch (start us, length us, event | category | flops | bytes accessed | tf_op | source)
XLA Modules:
  0.0 322.9 jit_solution(3960021001715610415)
XLA Ops:
  0.0 320.6 %shard_map.181 = bf16[1024,512]{1,0:T(8,128)(2,1)} custom-call(bf16[1024,512]{1,0:T(8,128)(2,1)} %tokens.1, bf16[256,1280]{1,0:T(8,128)(2,1)} %first_gate.1, bf16[256,1280]{1,0:T(8,128)(2,1)} %first_up.1, bf16[256,1280]{1,0:T(8,128)(2,1)} %first_down.1, bf16[256,256]{1,0:T(8,128)(2,1)} %mix_input.1, bf16[256,256]{1,0:T(8,128)(2,1)} %mix_branch.1, ...), custom_call_target="tpu_custom_call" | custom-call | flops 35433480192 | bytes 20971520 | tf_op jit(solution)/shard_map/pallas_call | solution.py:890
  320.6 2.3 copy.21
